TPU v7x, 32 devices: a whole 2x2x4 slice. The times are simulated.
32 devices in a mesh: fs: 8 (over z, x), tp: 4 (over y, core).
Axes of the slice: x: 2, y: 2, z: 4, core: 2. Of those that a mesh axis runs over, the one named last changes fastest.
Arguments:
- tokens: bfloat16 [4096, 2048], P('fs', 'tp'), may hold values from -6 to 6
- pre_gain: float32 [2048], replicated, may hold values from 0.1 to 1.9
- pre_gate: float32 [2048, 2816], P('fs', 'tp'), may hold values from -0.125 to 0.125
- pre_up: float32 [2048, 2816], P('fs', 'tp'), may hold values from -0.125 to 0.125
- pre_down: float32 [2816, 2048], P('fs', 'tp'), may hold values from -0.109375 to 0.109375
- mix_gain: float32 [2048], replicated, may hold values from 0.1 to 1.9
- branch_proj: float32 [2048, 1024], P('fs', 'tp'), may hold values from -0.125 to 0.125
- gate_proj: float32 [2048, 1024], P('fs', 'tp'), may hold values from -0.125 to 0.125
- conv_taps: float32 [4, 1024], P(None, 'tp'), may hold values from -3 to 3
- retain_blocks: float32 [16, 64, 64], P('tp'), may hold values from -0.75 to 0.75
- admit_blocks: float32 [16, 64, 64], P('tp'), may hold values from -0.75 to 0.75
- decay_param: float32 [1024], P('tp'), may hold values from 5 to 8.5
- channel_gain: float32 [1024], replicated, may hold values from 0.1 to 1.9
- out_proj: float32 [1024, 2048], P('fs', 'tp'), may hold values from -0.1875 to 0.1875
- post_gain: float32 [2048], replicated, may hold values from 0.1 to 1.9
- post_gate: float32 [2048, 2816], P('fs', 'tp'), may hold values from -0.125 to 0.125
- post_up: float32 [2048, 2816], P('fs', 'tp'), may hold values from -0.125 to 0.125
- post_down: float32 [2816, 2048], P('fs', 'tp'), may hold values from -0.109375 to 0.109375
Outputs:
- layer_out: bfloat16 [4096, 2048], P('fs', 'tp')
All inputs are finite; a program needn't handle non-finite values.
Results may differ from a plain program's by a relative error of at most 0.012.
Values may be sent and summed in bfloat16 or wider, within the bound.
A program may use at most 64 MiB of HBM per device.

v0:
```python
import jax
import jax.numpy as jnp
from jax import lax
from jax.sharding import PartitionSpec as P

SEQ_LEN = 128
EPSILON = 1e-06
DECAY_SCALE = 8.0


def normalize(values, norm_gain):
    floats = values.astype(jnp.float32)
    scaled = floats * lax.rsqrt(jnp.mean(floats * floats, axis=-1, keepdims=True) + EPSILON)
    return (scaled * norm_gain).astype(jnp.bfloat16)


def combine(earlier, latter):
    keep_early, add_early = earlier
    keep_late, add_late = latter
    return (keep_early * keep_late, keep_late * add_early + add_late)


def widen(residual):
    return lax.all_gather(residual, "tp", axis=1, tiled=True)


def contract(operand, stacked):
    return jnp.dot(
        operand,
        lax.all_gather(stacked.astype(jnp.bfloat16), "fs", axis=0, tiled=True),
        preferred_element_type=jnp.float32,
    )


def feed_forward(residual, norm_gain, gate_matrix, up_matrix, down_matrix):
    normed = normalize(widen(residual), norm_gain)
    products = contract(normed, jnp.concatenate((gate_matrix, up_matrix), axis=1))
    split_at = gate_matrix.shape[1]
    hidden = (jax.nn.silu(products[:, :split_at]) * products[:, split_at:]).astype(jnp.bfloat16)
    all_hidden = lax.all_gather(hidden, "tp", axis=1, tiled=True)
    return (residual.astype(jnp.float32) + 0.5 * contract(all_hidden, down_matrix)).astype(
        jnp.bfloat16
    )


def block_gate(convolved, blocks):
    grouped = convolved.reshape(
        convolved.shape[0], convolved.shape[1], blocks.shape[0], blocks.shape[1]
    )
    mixed = jnp.einsum(
        "sthi,hij->sthj", grouped, blocks.astype(jnp.bfloat16), preferred_element_type=jnp.float32
    )
    return jax.nn.sigmoid(mixed).reshape(convolved.shape)


def recurrent_mixer(
    residual,
    norm_gain,
    branch_matrix,
    gate_matrix,
    conv_taps,
    retain_blocks,
    admit_blocks,
    decay_param,
    channel_gain,
    out_matrix,
):
    normed = normalize(widen(residual), norm_gain)
    products = contract(normed, jnp.concatenate((branch_matrix, gate_matrix), axis=1))
    local_width = branch_matrix.shape[1]
    branch = products[:, :local_width]
    gate_act = products[:, local_width:]
    taps_count = conv_taps.shape[0]
    sequences = residual.shape[0] // SEQ_LEN
    framed = branch.reshape(sequences, SEQ_LEN, local_width)
    padded = jnp.pad(framed, ((0, 0), (taps_count - 1, 0), (0, 0)))
    convolved = jnp.zeros_like(framed)
    for tap_index in range(taps_count):
        convolved = convolved + padded[:, tap_index : tap_index + SEQ_LEN] * conv_taps[tap_index]
    convolved = convolved.astype(jnp.bfloat16)
    retained = block_gate(convolved, retain_blocks)
    admitted = block_gate(convolved, admit_blocks)
    log_keep = -DECAY_SCALE * retained * jax.nn.softplus(-decay_param)
    inject = jnp.sqrt(-jnp.expm1(2.0 * log_keep)) * admitted * convolved.astype(jnp.float32)
    _, states = lax.associative_scan(combine, (jnp.exp(log_keep), inject), axis=1)
    mixed_rows = (states.reshape(residual.shape[0], local_width) * jax.nn.gelu(gate_act)).astype(
        jnp.bfloat16
    )
    all_channels = lax.all_gather(mixed_rows, "tp", axis=1, tiled=True)
    mixed_normed = normalize(all_channels, channel_gain)
    return (residual.astype(jnp.float32) + contract(mixed_normed, out_matrix)).astype(jnp.bfloat16)


def local(
    tokens,
    pre_gain,
    pre_gate,
    pre_up,
    pre_down,
    mix_gain,
    branch_proj,
    gate_proj,
    conv_taps,
    retain_blocks,
    admit_blocks,
    decay_param,
    channel_gain,
    out_proj,
    post_gain,
    post_gate,
    post_up,
    post_down,
):
    after_pre = feed_forward(tokens, pre_gain, pre_gate, pre_up, pre_down)
    after_mix = recurrent_mixer(
        after_pre,
        mix_gain,
        branch_proj,
        gate_proj,
        conv_taps,
        retain_blocks,
        admit_blocks,
        decay_param,
        channel_gain,
        out_proj,
    )
    return feed_forward(after_mix, post_gain, post_gate, post_up, post_down)


def solution(mesh):
    placed = (
        P("fs", "tp"),
        P(),
        P("fs", "tp"),
        P("fs", "tp"),
        P("fs", "tp"),
        P(),
        P("fs", "tp"),
        P("fs", "tp"),
        P(None, "tp"),
        P("tp", None, None),
        P("tp", None, None),
        P("tp"),
        P(),
        P("fs", "tp"),
        P(),
        P("fs", "tp"),
        P("fs", "tp"),
        P("fs", "tp"),
    )
    return jax.shard_map(
        local, mesh=mesh, in_specs=placed, out_specs=P("fs", "tp"), check_vma=False
    )
```

profile of v0, /device:TPU:0, one launch (start us, length us, event | category | flops | bytes accessed | tf_op | source)
XLA Modules:
  0.0 807.1 jit_solution(914277624177452306)
XLA Ops:
  10.4 23.8 %all-gather.13.cloned.1.call-done = bf16[512,2048]{1,0:T(8,128)(2,1)} async-done(((bf16[512,512]{1,0:T(8,128)(2,1)}), bf16[512,2048]{1,0:T(8,128)(2,1)}) %all-gather.13.cloned.1.call-update) | async-done | bytes 2097168 | tf_op jit(solution)/shard_map/all_gather | solution.py:24
  36.5 93.0 %all-gather.15.cloned.1.call-done = bf16[2048,1408]{0,1:T(8,128)(2,1)} async-done(((bf16[256,1408]{0,1:T(8,128)(2,1)}), bf16[2048,1408]{0,1:T(8,128)(2,1)}) %all-gather.15.cloned.1.call-update) | async-done | bytes 5767184 | tf_op jit(solution)/shard_map/all_gather | solution.py:30
  129.4 5.8 fusion.16
  137.0 50.1 %all-gather.19.cloned.1.call-done = bf16[2816,512]{1,0:T(8,128)(2,1)} async-done(((bf16[352,512]{1,0:T(8,128)(2,1)}), bf16[2816,512]{1,0:T(8,128)(2,1)}) %all-gather.19.cloned.1.call-update) | async-done | bytes 2883600 | tf_op jit(solution)/shard_map/all_gather | solution.py:30
  187.1 27.1 %all-gather.17.cloned.1.call-done = bf16[512,2816]{0,1:T(8,128)(2,1)} async-done(((bf16[512,704]{0,1:T(8,128)(2,1)}), bf16[512,2816]{0,1:T(8,128)(2,1)}) %all-gather.17.cloned.1.call-update) | async-done | bytes 2883600 | tf_op jit(solution)/shard_map/all_gather | solution.py:40
  214.2 5.2 fusion.29
  220.4 21.7 %all-gather.21.cloned.1.call-done = bf16[512,2048]{1,0:T(8,128)(2,1)} async-done(((bf16[512,512]{1,0:T(8,128)(2,1)}), bf16[512,2048]{1,0:T(8,128)(2,1)}) %all-gather.21.cloned.1.call-update) | async-done | bytes 2097168 | tf_op jit(solution)/shard_map/all_gather | solution.py:24
  244.4 48.9 %all-gather.23.cloned.1.call-done = bf16[2048,512]{1,0:T(8,128)(2,1)} async-done(((bf16[256,512]{1,0:T(8,128)(2,1)}), bf16[2048,512]{1,0:T(8,128)(2,1)}) %all-gather.23.cloned.1.call-update) | async-done | bytes 2097168 | tf_op jit(solution)/shard_map/all_gather | solution.py:30
  299.5 9.1 %slice.212 = f32[4,64,256]{1,2,0:T(8,128)S(1)} slice(f32[4,128,256]{1,2,0:T(8,128)S(1)} %get-tuple-element.6), slice={[0:4:1], [0:127:2], [0:256:1]} | slice | bytes 524288 | tf_op jit(solution)/shard_map/slice | solution.py:85
  308.6 9.1 %slice.213 = f32[4,64,256]{1,2,0:T(8,128)S(1)} slice(f32[4,128,256]{1,2,0:T(8,128)S(1)} %get-tuple-element.6), slice={[0:4:1], [1:128:2], [0:256:1]} | slice | bytes 524288 | tf_op jit(solution)/shard_map/slice | solution.py:85
  317.6 9.1 %slice.211 = f32[4,64,256]{1,2,0:T(8,128)S(1)} slice(f32[4,128,256]{1,2,0:T(8,128)S(1)} %get-tuple-element.5), slice={[0:4:1], [1:128:2], [0:256:1]} | slice | bytes 524288 | tf_op jit(solution)/shard_map/slice | solution.py:85
  326.7 9.5 %slice.215 = f32[4,64,256]{1,2,0:T(8,128)} slice(f32[4,128,256]{1,2,0:T(8,128)S(1)} %get-tuple-element.5), slice={[0:4:1], [0:127:2], [0:256:1]} | slice | bytes 524288 | tf_op jit(solution)/shard_map/slice | solution.py:85
  337.4 4.6 slice.218
  342.0 4.7 slice.219
  346.7 5.3 slice.217
  352.1 5.2 slice.221
  426.2 6.1 slice.216
  432.2 5.2 slice.257
  437.4 9.5 %slice.259 = f32[4,63,256]{1,2,0:T(8,128)} slice(f32[4,128,256]{1,2,0:T(8,128)S(1)} %get-tuple-element.6), slice={[0:4:1], [2:128:2], [0:256:1]} | slice | bytes 516096 | tf_op jit(solution)/shard_map/slice | solution.py:85
  446.9 9.9 %slice.210 = f32[4,63,256]{1,2,0:T(8,128)} slice(f32[4,128,256]{1,2,0:T(8,128)S(1)} %copy-done.1), slice={[0:4:1], [2:128:2], [0:256:1]} | slice | bytes 516096 | tf_op jit(solution)/shard_map/slice | solution.py:85
  502.3 4.5 pad.58
  506.8 4.6 pad.59
  512.3 9.8 %pad.61 = f32[4,128,256]{1,2,0:T(8,128)S(1)} pad(f32[4,64,256]{1,2,0:T(8,128)} %add.195, f32[]{:T(128)} %constant.10.clone.1), padding=0_0_0x1_0_1x0_0_0 | pad | bytes 786436 | tf_op jit(solution)/shard_map/pad | solution.py:85
  522.5 8.8 %pad.60 = f32[4,128,256]{1,2,0:T(8,128)S(1)} pad(f32[4,64,256]{1,2,0:T(8,128)S(1)} %pad_maximum_fusion.4, f32[]{:T(128)} %constant.10.clone.1), padding=0_0_0x0_1_1x0_0_0 | pad | bytes 786436 | tf_op jit(solution)/shard_map/pad | solution.py:85
  533.3 14.7 %all-gather.25.cloned.1.call-done = bf16[512,1024]{1,0:T(8,128)(2,1)} async-done(((bf16[512,256]{1,0:T(8,128)(2,1)}), bf16[512,1024]{1,0:T(8,128)(2,1)}) %all-gather.25.cloned.1.call-update) | async-done | bytes 1048592 | tf_op jit(solution)/shard_map/all_gather | solution.py:89
  549.6 40.9 %all-gather.27.cloned.1.call-done = bf16[1024,512]{1,0:T(8,128)(2,1)} async-done(((bf16[128,512]{1,0:T(8,128)(2,1)}), bf16[1024,512]{1,0:T(8,128)(2,1)}) %all-gather.27.cloned.1.call-update) | async-done | bytes 1048592 | tf_op jit(solution)/shard_map/all_gather | solution.py:30
  595.8 19.2 %all-gather.29.cloned.1.call-done = bf16[512,2048]{1,0:T(8,128)(2,1)} async-done(((bf16[512,512]{1,0:T(8,128)(2,1)}), bf16[512,2048]{1,0:T(8,128)(2,1)}) %all-gather.29.cloned.1.call-update) | async-done | bytes 2097168 | tf_op jit(solution)/shard_map/all_gather | solution.py:24
  617.3 92.8 %all-gather.31.cloned.1.call-done = bf16[2048,1408]{0,1:T(8,128)(2,1)} async-done(((bf16[256,1408]{0,1:T(8,128)(2,1)}), bf16[2048,1408]{0,1:T(8,128)(2,1)}) %all-gather.31.cloned.1.call-update) | async-done | bytes 5767184 | tf_op jit(solution)/shard_map/all_gather | solution.py:30
  710.1 5.8 fusion.12
  717.6 50.2 %all-gather.35.cloned.1.call-done = bf16[2816,512]{1,0:T(8,128)(2,1)} async-done(((bf16[352,512]{1,0:T(8,128)(2,1)}), bf16[2816,512]{1,0:T(8,128)(2,1)}) %all-gather.35.cloned.1.call-update) | async-done | bytes 2883600 | tf_op jit(solution)/shard_map/all_gather | solution.py:30
  767.8 27.1 %all-gather.33.cloned.1.call-done = bf16[512,2816]{0,1:T(8,128)(2,1)} async-done(((bf16[512,704]{0,1:T(8,128)(2,1)}), bf16[512,2816]{0,1:T(8,128)(2,1)}) %all-gather.33.cloned.1.call-update) | async-done | bytes 2883600 | tf_op jit(solution)/shard_map/all_gather | solution.py:40
  794.9 5.2 fusion.28
  (213 shorter events, 146.2 us)
Async XLA Ops:
  6.5 27.7 %all-gather.13.cloned.1.call-start = ((), (), s32[]{:S(2)}) async-start(), calls=%async_computation | async-start | bytes 2621440 | tf_op jit(solution)/shard_map/all_gather | solution.py:24
  7.3 122.1 %all-gather.15.cloned.1.call-start = ((), (), s32[]{:S(2)}) async-start(), calls=%async_computation.1 | async-start | bytes 6488064 | tf_op jit(solution)/shard_map/all_gather | solution.py:30
  9.5 119.9 %copy-start.36 = (f32[2048]{0:T(1024)S(1)}, f32[2048]{0:T(1024)}, u32[]{:S(2)}) copy-start(f32[2048]{0:T(1024)} %param.19) | copy-start | bytes 24580
  9.5 177.6 %all-gather.19.cloned.1.call-start = ((), (), s32[]{:S(2)}) async-start(), calls=%async_computation.3 | async-start | bytes 3244032 | tf_op jit(solution)/shard_map/all_gather | solution.py:30
  10.4 203.8 %all-gather.17.cloned.1.call-start = ((), (), s32[]{:S(2)}) async-start(), calls=%async_computation.2 | async-start | bytes 3604480 | tf_op jit(solution)/shard_map/all_gather | solution.py:40
  34.2 95.2 %copy-start.14 = (bf16[512,2048]{1,0:T(8,128)(2,1)S(1)}, bf16[512,2048]{1,0:T(8,128)(2,1)}, u32[]{:S(2)}) copy-start(bf16[512,2048]{1,0:T(8,128)(2,1)} %all-gather.13.cloned.1.call-done) | copy-start | bytes 6291460
  135.8 78.4 %copy-start.26 = (bf16[512,512]{1,0:T(8,128)(2,1)S(1)}, bf16[512,512]{1,0:T(8,128)(2,1)}, u32[]{:S(2)}) copy-start(bf16[512,512]{1,0:T(8,128)(2,1)} %param.18) | copy-start | bytes 1572868
  136.9 82.5 %copy-start.29 = (f32[256,256]{1,0:T(8,128)S(1)}, f32[256,256]{1,0:T(8,128)}, u32[]{:S(2)}) copy-start(f32[256,256]{1,0:T(8,128)} %param.24) | copy-start | bytes 786436
  137.0 82.5 %copy-start.30 = (f32[256,256]{1,0:T(8,128)S(1)}, f32[256,256]{1,0:T(8,128)}, u32[]{:S(2)}) copy-start(f32[256,256]{1,0:T(8,128)} %param.25) | copy-start | bytes 786436
  137.0 105.2 %all-gather.21.cloned.1.call-start = ((), (), s32[]{:S(2)}) async-start(), calls=%async_computation.4 | async-start | bytes 2621440 | tf_op jit(solution)/shard_map/all_gather | solution.py:24
  219.4 73.8 %copy-start.37 = (f32[2048]{0:T(1024)S(1)}, f32[2048]{0:T(1024)}, u32[]{:S(2)}) copy-start(f32[2048]{0:T(1024)} %param.23) | copy-start | bytes 24580
  219.4 73.8 %all-gather.23.cloned.1.call-start = ((), (), s32[]{:S(2)}) async-start(), calls=%async_computation.5 | async-start | bytes 2359296 | tf_op jit(solution)/shard_map/all_gather | solution.py:30
  220.3 327.7 %all-gather.25.cloned.1.call-start = ((), (), s32[]{:S(2)}) async-start(), calls=%async_computation.6 | async-start | bytes 1310720 | tf_op jit(solution)/shard_map/all_gather | solution.py:89
  242.1 51.1 %copy-start.16 = (bf16[512,2048]{1,0:T(8,128)(2,1)S(1)}, bf16[512,2048]{1,0:T(8,128)(2,1)}, u32[]{:S(2)}) copy-start(bf16[512,2048]{1,0:T(8,128)(2,1)} %all-gather.21.cloned.1.call-done) | copy-start | bytes 6291460
  299.4 27.2 %copy-start = (f32[4,128,256]{1,2,0:T(8,128)}, f32[4,128,256]{1,2,0:T(8,128)S(1)}, u32[]{:S(2)}) copy-start(f32[4,128,256]{1,2,0:T(8,128)S(1)} %get-tuple-element.5) | copy-start | bytes 1572868
  337.4 14.7 %copy-start.2 = (f32[4,64,256]{1,2,0:T(8,128)}, f32[4,64,256]{1,2,0:T(8,128)S(1)}, u32[]{:S(2)}) copy-start(f32[4,64,256]{1,2,0:T(8,128)S(1)} %get-tuple-element.19) | copy-start | bytes 786436
  408.7 11.4 %copy-start.4 = (f32[4,32,256]{1,2,0:T(8,128)S(1)}, f32[4,32,256]{1,2,0:T(8,128)}, u32[]{:S(2)}) copy-start(f32[4,32,256]{1,2,0:T(8,128)} %copy-done.3) | copy-start | bytes 393220
  423.1 23.8 %copy-start.1 = (f32[4,128,256]{1,2,0:T(8,128)S(1)}, f32[4,128,256]{1,2,0:T(8,128)}, u32[]{:S(2)}) copy-start(f32[4,128,256]{1,2,0:T(8,128)} %copy-done) | copy-start | bytes 1572868
  506.8 15.3 %copy-start.10 = (f32[4,63,256]{1,2,0:T(8,128)S(1)}, f32[4,63,256]{1,2,0:T(8,128)}, u32[]{:S(2)}) copy-start(f32[4,63,256]{1,2,0:T(8,128)} %slice.259) | copy-start | bytes 774148
  506.8 15.3 %copy-start.11 = (f32[4,63,256]{1,2,0:T(8,128)S(1)}, f32[4,63,256]{1,2,0:T(8,128)}, u32[]{:S(2)}) copy-start(f32[4,63,256]{1,2,0:T(8,128)} %slice.210) | copy-start | bytes 774148
  531.4 59.1 %copy-start.27 = (bf16[512,512]{1,0:T(8,128)(2,1)S(1)}, bf16[512,512]{1,0:T(8,128)(2,1)}, u32[]{:S(2)}) copy-start(bf16[512,512]{1,0:T(8,128)(2,1)} %fusion.29) | copy-start | bytes 1572868
  531.4 59.1 %copy-start.39 = (f32[1024]{0:T(1024)S(1)}, f32[1024]{0:T(1024)}, u32[]{:S(2)}) copy-start(f32[1024]{0:T(1024)} %param.30) | copy-start | bytes 12292
  532.5 57.9 %all-gather.27.cloned.1.call-start = ((), (), s32[]{:S(2)}) async-start(), calls=%async_computation.7 | async-start | bytes 1179648 | tf_op jit(solution)/shard_map/all_gather | solution.py:30
  533.3 81.7 %all-gather.29.cloned.1.call-start = ((), (), s32[]{:S(2)}) async-start(), calls=%async_computation.8 | async-start | bytes 2621440 | tf_op jit(solution)/shard_map/all_gather | solution.py:24
  549.5 44.3 %copy-start.23 = (f32[256,704]{0,1:T(8,128)S(1)}, f32[256,704]{0,1:T(8,128)}, u32[]{:S(2)}) copy-start(f32[256,704]{0,1:T(8,128)} %param.33) | copy-start | bytes 2162692
  549.6 44.3 %copy-start.24 = (f32[256,704]{0,1:T(8,128)S(1)}, f32[256,704]{0,1:T(8,128)}, u32[]{:S(2)}) copy-start(f32[256,704]{0,1:T(8,128)} %param.34) | copy-start | bytes 2162692
  593.6 116.5 %all-gather.31.cloned.1.call-start = ((), (), s32[]{:S(2)}) async-start(), calls=%async_computation.9 | async-start | bytes 6488064 | tf_op jit(solution)/shard_map/all_gather | solution.py:30
  594.9 115.2 %copy-start.38 = (f32[2048]{0:T(1024)S(1)}, f32[2048]{0:T(1024)}, u32[]{:S(2)}) copy-start(f32[2048]{0:T(1024)} %param.32) | copy-start | bytes 24580
  594.9 172.9 %all-gather.35.cloned.1.call-start = ((), (), s32[]{:S(2)}) async-start(), calls=%async_computation.11 | async-start | bytes 3244032 | tf_op jit(solution)/shard_map/all_gather | solution.py:30
  595.8 199.1 %all-gather.33.cloned.1.call-start = ((), (), s32[]{:S(2)}) async-start(), calls=%async_computation.10 | async-start | bytes 3604480 | tf_op jit(solution)/shard_map/all_gather | solution.py:40
  615.0 95.1 %copy-start.15 = (bf16[512,2048]{1,0:T(8,128)(2,1)S(1)}, bf16[512,2048]{1,0:T(8,128)(2,1)}, u32[]{:S(2)}) copy-start(bf16[512,2048]{1,0:T(8,128)(2,1)} %all-gather.29.cloned.1.call-done) | copy-start | bytes 6291460
  716.4 78.5 %copy-start.28 = (bf16[512,512]{1,0:T(8,128)(2,1)S(1)}, bf16[512,512]{1,0:T(8,128)(2,1)}, u32[]{:S(2)}) copy-start(bf16[512,512]{1,0:T(8,128)(2,1)} %fusion.30) | copy-start | bytes 1572868
  (20 other events, 68.0 us)
Sparse Core Ops, SparseCore 0:
  8.9 25.2 all-gather.12
  36.3 93.1 all-gather.14
  131.6 55.4 all-gather.18
  188.5 25.6 all-gather.16
  219.5 22.5 all-gather.20
  244.1 49.0 all-gather.22
  532.6 15.3 all-gather.24
  550.2 40.2 all-gather.26
  593.7 21.2 all-gather.28
  616.9 93.1 all-gather.30
  712.3 55.4 all-gather.34
  769.2 25.6 all-gather.32
where the time goes:
time: 815 us; the launch traced here: 807 us
  waiting for transfers between devices  510 us (63%)
  local copies, waits for them, and re-layouts  210 us (26%)
  other arithmetic  42.7 us (5%)
  matrix products  28.7 us (4%)
  between operations  14.5 us (2%)
    all_gather x6, waiting for transfers between devices, contract(): lax.all_gather(stacked.astype(jnp.bfloat16), 'fs', axis=0, tiled=True)  376 us
    slice x34, local copies, waits for them, and re-layouts, recurrent_mixer(): lax.associative_scan(combine, (jnp.exp(log_keep), inject), axis=1)  144 us
    all_gather x3, waiting for transfers between devices, widen(): return lax.all_gather(residual, 'tp', axis=1, tiled=True)  64.7 us
    all_gather x2, waiting for transfers between devices, feed_forward(): all_hidden = lax.all_gather(hidden, 'tp', axis=1, tiled=True)  54.2 us
    pad x12, local copies, waits for them, and re-layouts, recurrent_mixer(): lax.associative_scan(combine, (jnp.exp(log_keep), inject), axis=1)  50.5 us
    dot_general x6, matrix products, contract(): jnp.dot(operand, lax.all_gather(stacked.astype(jnp.bfloat16), 'fs', axis=...  28 us
  transfers between devices with their start and end apart: 12, of which 12 were waited for; matrix products, arithmetic and copies ran while one was open for 4% of the time, Pallas kernels for 0%

commit v1 on v0

--- a/solution.py
+++ b/solution.py
@@ -37,7 +37,8 @@
     products = contract(normed, jnp.concatenate((gate_matrix, up_matrix), axis=1))
     split_at = gate_matrix.shape[1]
     hidden = (jax.nn.silu(products[:, :split_at]) * products[:, split_at:]).astype(jnp.bfloat16)
-    all_hidden = lax.all_gather(hidden, "tp", axis=1, tiled=True)
+    tiles = lax.all_gather(hidden, "tp")
+    all_hidden = jnp.concatenate(tiles, axis=1)
     return (residual.astype(jnp.float32) + 0.5 * contract(all_hidden, down_matrix)).astype(
         jnp.bfloat16
     )

time: 815 us -> 832 us (1.021)
    all_gather x6, waiting for transfers between devices: 376 us -> 388 us  [contract(): lax.all_gather(stacked.astype(jnp.bfloat16), 'fs', axis=0, tiled=True)]
  transfers between devices with their start and end apart: 12 -> 12, of which waited for: 12 -> 12; matrix products, arithmetic and copies ran while one was open for 4% -> 3% of each run, Pallas kernels for 0% -> 0%
where the time goes in v1:
time: 832 us; the launch traced here: 824 us
  waiting for transfers between devices  518 us (62%)
  local copies, waits for them, and re-layouts  213 us (26%)
  other arithmetic  48.5 us (6%)
  matrix products  28.9 us (3%)
  between operations  14.5 us (2%)
    all_gather x6, waiting for transfers between devices, contract(): lax.all_gather(stacked.astype(jnp.bfloat16), 'fs', axis=0, tiled=True)  388 us
    slice x34, local copies, waits for them, and re-layouts, recurrent_mixer(): lax.associative_scan(combine, (jnp.exp(log_keep), inject), axis=1)  144 us
    all_gather x3, waiting for transfers between devices, widen(): return lax.all_gather(residual, 'tp', axis=1, tiled=True)  62.1 us
    all_gather x2, waiting for transfers between devices, feed_forward(): tiles = lax.all_gather(hidden, 'tp')  51.9 us
    pad x12, local copies, waits for them, and re-layouts, recurrent_mixer(): lax.associative_scan(combine, (jnp.exp(log_keep), inject), axis=1)  50.4 us
    dot_general x6, matrix products, contract(): jnp.dot(operand, lax.all_gather(stacked.astype(jnp.bfloat16), 'fs', axis=...  28.2 us
  transfers between devices with their start and end apart: 12, of which 12 were waited for; matrix products, arithmetic and copies ran while one was open for 3% of the time, Pallas kernels for 0%

profile of v1, /device:TPU:0, one launch (start us, length us, event | category | flops | bytes accessed | tf_op | source)
XLA Modules:
  0.0 823.7 jit_solution(8854822473263605013)
XLA Ops:
  10.7 23.5 %all-gather.15.cloned.1.call-done = bf16[512,2048]{1,0:T(8,128)(2,1)} async-done(((bf16[512,512]{1,0:T(8,128)(2,1)}), bf16[512,2048]{1,0:T(8,128)(2,1)}) %all-gather.15.cloned.1.call-update) | async-done | bytes 2097168 | tf_op jit(solution)/shard_map/all_gather | solution.py:24
  36.3 93.1 %all-gather.17.cloned.1.call-done = bf16[2048,1408]{0,1:T(8,128)(2,1)} async-done(((bf16[256,1408]{0,1:T(8,128)(2,1)}), bf16[2048,1408]{0,1:T(8,128)(2,1)}) %all-gather.17.cloned.1.call-update) | async-done | bytes 5767184 | tf_op jit(solution)/shard_map/all_gather | solution.py:30
  129.4 6.5 fusion.16
  138.4 25.9 %all-gather.35.cloned.1.call-done = bf16[2048,704]{1,0:T(8,128)(2,1)} async-done(((bf16[512,704]{1,0:T(8,128)(2,1)}), bf16[2048,704]{1,0:T(8,128)(2,1)}) %all-gather.35.cloned.1.call-update) | async-done | bytes 2883600 | tf_op jit(solution)/shard_map/all_gather | solution.py:40
  167.5 56.2 %all-gather.19.cloned.1.call-done = bf16[2816,512]{1,0:T(8,128)(2,1)} async-done(((bf16[352,512]{1,0:T(8,128)(2,1)}), bf16[2816,512]{1,0:T(8,128)(2,1)}) %all-gather.19.cloned.1.call-update) | async-done | bytes 2883600 | tf_op jit(solution)/shard_map/all_gather | solution.py:30
  223.7 4.3 fusion.29
  230.9 18.5 %all-gather.21.cloned.1.call-done = bf16[512,2048]{1,0:T(8,128)(2,1)} async-done(((bf16[512,512]{1,0:T(8,128)(2,1)}), bf16[512,2048]{1,0:T(8,128)(2,1)}) %all-gather.21.cloned.1.call-update) | async-done | bytes 2097168 | tf_op jit(solution)/shard_map/all_gather | solution.py:24
  251.5 49.0 %all-gather.23.cloned.1.call-done = bf16[2048,512]{1,0:T(8,128)(2,1)} async-done(((bf16[256,512]{1,0:T(8,128)(2,1)}), bf16[2048,512]{1,0:T(8,128)(2,1)}) %all-gather.23.cloned.1.call-update) | async-done | bytes 2097168 | tf_op jit(solution)/shard_map/all_gather | solution.py:30
  307.4 9.1 %slice.212 = f32[4,64,256]{1,2,0:T(8,128)S(1)} slice(f32[4,128,256]{1,2,0:T(8,128)S(1)} %get-tuple-element.6), slice={[0:4:1], [0:127:2], [0:256:1]} | slice | bytes 524288 | tf_op jit(solution)/shard_map/slice | solution.py:86
  316.5 9.1 %slice.213 = f32[4,64,256]{1,2,0:T(8,128)S(1)} slice(f32[4,128,256]{1,2,0:T(8,128)S(1)} %get-tuple-element.6), slice={[0:4:1], [1:128:2], [0:256:1]} | slice | bytes 524288 | tf_op jit(solution)/shard_map/slice | solution.py:86
  325.5 9.1 %slice.211 = f32[4,64,256]{1,2,0:T(8,128)S(1)} slice(f32[4,128,256]{1,2,0:T(8,128)S(1)} %get-tuple-element.5), slice={[0:4:1], [1:128:2], [0:256:1]} | slice | bytes 524288 | tf_op jit(solution)/shard_map/slice | solution.py:86
  334.6 9.5 %slice.215 = f32[4,64,256]{1,2,0:T(8,128)} slice(f32[4,128,256]{1,2,0:T(8,128)S(1)} %get-tuple-element.5), slice={[0:4:1], [0:127:2], [0:256:1]} | slice | bytes 524288 | tf_op jit(solution)/shard_map/slice | solution.py:86
  345.3 4.6 slice.218
  349.9 4.7 slice.219
  354.6 5.3 slice.217
  360.0 5.2 slice.221
  426.9 4.3 slice.222
  434.3 6.1 slice.216
  440.3 5.2 slice.257
  445.5 9.5 %slice.259 = f32[4,63,256]{1,2,0:T(8,128)} slice(f32[4,128,256]{1,2,0:T(8,128)S(1)} %get-tuple-element.6), slice={[0:4:1], [2:128:2], [0:256:1]} | slice | bytes 516096 | tf_op jit(solution)/shard_map/slice | solution.py:86
  455.0 9.9 %slice.210 = f32[4,63,256]{1,2,0:T(8,128)} slice(f32[4,128,256]{1,2,0:T(8,128)S(1)} %copy-done.1), slice={[0:4:1], [2:128:2], [0:256:1]} | slice | bytes 516096 | tf_op jit(solution)/shard_map/slice | solution.py:86
  510.3 4.5 pad.58
  514.8 4.6 pad.59
  520.3 9.8 %pad.61 = f32[4,128,256]{1,2,0:T(8,128)S(1)} pad(f32[4,64,256]{1,2,0:T(8,128)} %add.195, f32[]{:T(128)} %constant.10.clone.1), padding=0_0_0x1_0_1x0_0_0 | pad | bytes 786436 | tf_op jit(solution)/shard_map/pad | solution.py:86
  530.5 8.8 %pad.60 = f32[4,128,256]{1,2,0:T(8,128)S(1)} pad(f32[4,64,256]{1,2,0:T(8,128)S(1)} %pad_maximum_fusion.4, f32[]{:T(128)} %constant.10.clone.1), padding=0_0_0x0_1_1x0_0_0 | pad | bytes 786436 | tf_op jit(solution)/shard_map/pad | solution.py:86
  541.4 14.7 %all-gather.25.cloned.1.call-done = bf16[512,1024]{1,0:T(8,128)(2,1)} async-done(((bf16[512,256]{1,0:T(8,128)(2,1)}), bf16[512,1024]{1,0:T(8,128)(2,1)}) %all-gather.25.cloned.1.call-update) | async-done | bytes 1048592 | tf_op jit(solution)/shard_map/all_gather | solution.py:90
  557.6 40.9 %all-gather.27.cloned.1.call-done = bf16[1024,512]{1,0:T(8,128)(2,1)} async-done(((bf16[128,512]{1,0:T(8,128)(2,1)}), bf16[1024,512]{1,0:T(8,128)(2,1)}) %all-gather.27.cloned.1.call-update) | async-done | bytes 1048592 | tf_op jit(solution)/shard_map/all_gather | solution.py:30
  603.0 20.0 %all-gather.29.cloned.1.call-done = bf16[512,2048]{1,0:T(8,128)(2,1)} async-done(((bf16[512,512]{1,0:T(8,128)(2,1)}), bf16[512,2048]{1,0:T(8,128)(2,1)}) %all-gather.29.cloned.1.call-update) | async-done | bytes 2097168 | tf_op jit(solution)/shard_map/all_gather | solution.py:24
  625.1 93.0 %all-gather.31.cloned.1.call-done = bf16[2048,1408]{0,1:T(8,128)(2,1)} async-done(((bf16[256,1408]{0,1:T(8,128)(2,1)}), bf16[2048,1408]{0,1:T(8,128)(2,1)}) %all-gather.31.cloned.1.call-update) | async-done | bytes 5767184 | tf_op jit(solution)/shard_map/all_gather | solution.py:30
  718.1 6.5 fusion.12
  727.0 26.0 %all-gather.37.cloned.1.call-done = bf16[2048,704]{1,0:T(8,128)(2,1)} async-done(((bf16[512,704]{1,0:T(8,128)(2,1)}), bf16[2048,704]{1,0:T(8,128)(2,1)}) %all-gather.37.cloned.1.call-update) | async-done | bytes 2883600 | tf_op jit(solution)/shard_map/all_gather | solution.py:40
  756.2 56.2 %all-gather.33.cloned.1.call-done = bf16[2816,512]{1,0:T(8,128)(2,1)} async-done(((bf16[352,512]{1,0:T(8,128)(2,1)}), bf16[2816,512]{1,0:T(8,128)(2,1)}) %all-gather.33.cloned.1.call-update) | async-done | bytes 2883600 | tf_op jit(solution)/shard_map/all_gather | solution.py:30
  (197 shorter events, 155.6 us)
Async XLA Ops:
  6.5 27.7 %all-gather.15.cloned.1.call-start = ((), (), s32[]{:S(2)}) async-start(), calls=%async_computation | async-start | bytes 2621440 | tf_op jit(solution)/shard_map/all_gather | solution.py:24
  7.3 122.2 %all-gather.17.cloned.1.call-start = ((), (), s32[]{:S(2)}) async-start(), calls=%async_computation.1 | async-start | bytes 6488064 | tf_op jit(solution)/shard_map/all_gather | solution.py:30
  8.5 121.0 %copy-start.28 = (f32[2048]{0:T(1024)S(1)}, f32[2048]{0:T(1024)}, u32[]{:S(2)}) copy-start(f32[2048]{0:T(1024)} %param.19) | copy-start | bytes 24580
  10.6 153.7 %all-gather.35.cloned.1.call-start = ((), (), s32[]{:S(2)}) async-start(), calls=%async_computation.10 | async-start | bytes 3932160 | tf_op jit(solution)/shard_map/all_gather | solution.py:40
  137.5 86.2 %all-gather.19.cloned.1.call-start = ((), (), s32[]{:S(2)}) async-start(), calls=%async_computation.2 | async-start | bytes 3244032 | tf_op jit(solution)/shard_map/all_gather | solution.py:30
  138.4 111.0 %all-gather.21.cloned.1.call-start = ((), (), s32[]{:S(2)}) async-start(), calls=%async_computation.3 | async-start | bytes 2621440 | tf_op jit(solution)/shard_map/all_gather | solution.py:24
  164.3 59.4 %copy-start.20 = (bf16[512,512]{1,0:T(8,128)(2,1)S(1)}, bf16[512,512]{1,0:T(8,128)(2,1)}, u32[]{:S(2)}) copy-start(bf16[512,512]{1,0:T(8,128)(2,1)} %param.18) | copy-start | bytes 1572868
  223.7 7.1 copy-start.25
  223.7 7.2 copy-start.24
  228.0 72.5 %copy-start.29 = (f32[2048]{0:T(1024)S(1)}, f32[2048]{0:T(1024)}, u32[]{:S(2)}) copy-start(f32[2048]{0:T(1024)} %param.23) | copy-start | bytes 24580
  228.1 72.4 %all-gather.23.cloned.1.call-start = ((), (), s32[]{:S(2)}) async-start(), calls=%async_computation.4 | async-start | bytes 2359296 | tf_op jit(solution)/shard_map/all_gather | solution.py:30
  230.8 325.2 %all-gather.25.cloned.1.call-start = ((), (), s32[]{:S(2)}) async-start(), calls=%async_computation.5 | async-start | bytes 1310720 | tf_op jit(solution)/shard_map/all_gather | solution.py:90
  307.3 27.2 %copy-start = (f32[4,128,256]{1,2,0:T(8,128)}, f32[4,128,256]{1,2,0:T(8,128)S(1)}, u32[]{:S(2)}) copy-start(f32[4,128,256]{1,2,0:T(8,128)S(1)} %get-tuple-element.5) | copy-start | bytes 1572868
  345.3 14.7 %copy-start.2 = (f32[4,64,256]{1,2,0:T(8,128)}, f32[4,64,256]{1,2,0:T(8,128)S(1)}, u32[]{:S(2)}) copy-start(f32[4,64,256]{1,2,0:T(8,128)S(1)} %get-tuple-element.19) | copy-start | bytes 786436
  366.5 9.0 %copy-start.3 = (f32[4,32,256]{1,2,0:T(8,128)}, f32[4,32,256]{1,2,0:T(8,128)S(1)}, u32[]{:S(2)}) copy-start(f32[4,32,256]{1,2,0:T(8,128)S(1)} %get-tuple-element.17) | copy-start | bytes 393220
  380.0 7.0 copy-start.4
  426.9 28.1 %copy-start.1 = (f32[4,128,256]{1,2,0:T(8,128)S(1)}, f32[4,128,256]{1,2,0:T(8,128)}, u32[]{:S(2)}) copy-start(f32[4,128,256]{1,2,0:T(8,128)} %copy-done) | copy-start | bytes 1572868
  510.1 20.1 %copy-start.9 = (f32[4,63,256]{1,2,0:T(8,128)S(1)}, f32[4,63,256]{1,2,0:T(8,128)}, u32[]{:S(2)}) copy-start(f32[4,63,256]{1,2,0:T(8,128)} %slice.259) | copy-start | bytes 774148
  510.1 20.1 %copy-start.10 = (f32[4,63,256]{1,2,0:T(8,128)S(1)}, f32[4,63,256]{1,2,0:T(8,128)}, u32[]{:S(2)}) copy-start(f32[4,63,256]{1,2,0:T(8,128)} %slice.210) | copy-start | bytes 774148
  530.3 9.3 %copy-start.15 = (f32[512,512]{1,0:T(8,128)S(1)}, f32[512,512]{1,0:T(8,128)}, u32[]{:S(2)}) copy-start(f32[512,512]{1,0:T(8,128)} %copy-done.14) | copy-start | bytes 3145732
  530.5 10.1 %copy-start.23 = (f32[128,512]{1,0:T(8,128)S(1)}, f32[128,512]{1,0:T(8,128)}, u32[]{:S(2)}) copy-start(f32[128,512]{1,0:T(8,128)} %param.31) | copy-start | bytes 786436
  539.3 59.2 %copy-start.31 = (f32[1024]{0:T(1024)S(1)}, f32[1024]{0:T(1024)}, u32[]{:S(2)}) copy-start(f32[1024]{0:T(1024)} %param.30) | copy-start | bytes 12292
  539.4 59.1 %copy-start.21 = (bf16[512,512]{1,0:T(8,128)(2,1)S(1)}, bf16[512,512]{1,0:T(8,128)(2,1)}, u32[]{:S(2)}) copy-start(bf16[512,512]{1,0:T(8,128)(2,1)} %fusion.29) | copy-start | bytes 1572868
  540.5 57.9 %all-gather.27.cloned.1.call-start = ((), (), s32[]{:S(2)}) async-start(), calls=%async_computation.6 | async-start | bytes 1179648 | tf_op jit(solution)/shard_map/all_gather | solution.py:30
  541.3 60.5 %copy-start.17 = (f32[256,704]{0,1:T(8,128)S(1)}, f32[256,704]{0,1:T(8,128)}, u32[]{:S(2)}) copy-start(f32[256,704]{0,1:T(8,128)} %param.33) | copy-start | bytes 2162692
  541.3 81.7 %all-gather.29.cloned.1.call-start = ((), (), s32[]{:S(2)}) async-start(), calls=%async_computation.7 | async-start | bytes 2621440 | tf_op jit(solution)/shard_map/all_gather | solution.py:24
  557.6 44.3 %copy-start.18 = (f32[256,704]{0,1:T(8,128)S(1)}, f32[256,704]{0,1:T(8,128)}, u32[]{:S(2)}) copy-start(f32[256,704]{0,1:T(8,128)} %param.34) | copy-start | bytes 2162692
  601.6 116.5 %all-gather.31.cloned.1.call-start = ((), (), s32[]{:S(2)}) async-start(), calls=%async_computation.8 | async-start | bytes 6488064 | tf_op jit(solution)/shard_map/all_gather | solution.py:30
  601.9 116.2 %copy-start.30 = (f32[2048]{0:T(1024)S(1)}, f32[2048]{0:T(1024)}, u32[]{:S(2)}) copy-start(f32[2048]{0:T(1024)} %param.32) | copy-start | bytes 24580
  603.0 150.1 %all-gather.37.cloned.1.call-start = ((), (), s32[]{:S(2)}) async-start(), calls=%async_computation.11 | async-start | bytes 3932160 | tf_op jit(solution)/shard_map/all_gather | solution.py:40
  726.2 86.2 %all-gather.33.cloned.1.call-start = ((), (), s32[]{:S(2)}) async-start(), calls=%async_computation.9 | async-start | bytes 3244032 | tf_op jit(solution)/shard_map/all_gather | solution.py:30
  753.0 59.4 %copy-start.22 = (bf16[512,512]{1,0:T(8,128)(2,1)S(1)}, bf16[512,512]{1,0:T(8,128)(2,1)}, u32[]{:S(2)}) copy-start(bf16[512,512]{1,0:T(8,128)(2,1)} %fusion.30) | copy-start | bytes 1572868
  (12 other events, 42.6 us)
Sparse Core Ops, SparseCore 0:
  8.9 25.2 all-gather.14
  36.3 93.1 all-gather.16
  137.6 26.6 all-gather.34
  166.4 57.2 all-gather.18
  228.2 21.1 all-gather.20
  251.4 49.0 all-gather.22
  540.6 15.3 all-gather.24
  558.2 40.2 all-gather.26
  601.7 21.2 all-gather.28
  624.9 93.1 all-gather.30
  726.3 26.6 all-gather.36
  755.1 57.2 all-gather.32
